TPU v7x, 128 devices: a whole 4x4x4 slice. The times are simulated.
128 devices in a mesh: ep: 128 (over z, y, x, core).
Axes of the slice: x: 4, y: 4, z: 4, core: 2. Of those that a mesh axis runs over, the one named last changes fastest.
Arguments:
- tokens: bfloat16 [3072, 2048], P('ep'), may hold values from -6 to 6
- lengths: int32 [3072], P('ep'), may hold values from 2 to 1024
- latent_cache: bfloat16 [3072, 1024, 256], P('ep'), may hold values from -500 to 500
- rotary_cache: bfloat16 [3072, 1024, 32], P('ep'), may hold values from -6 to 6
- route_ids: int32 [3072, 6], P('ep'), may hold values from 0 to 127, all different within a row; in each aligned block of 24 rows (0 to 23, 24 to 47, ...) at most 3 rows name the same one
- route_scores: float32 [3072, 6], P('ep'), may hold values from 0.05 to 1
- attn_gain: bfloat16 [2048], replicated, may hold values from 0.099609375 to 1.8984375
- w_query_down: bfloat16 [2048, 256], replicated, may hold values from -0.125 to 0.125
- query_gain: bfloat16 [256], replicated, may hold values from 0.099609375 to 1.8984375
- w_query_nope: bfloat16 [256, 2048], replicated, may hold values from -0.375 to 0.375
- w_query_rope: bfloat16 [256, 1024], replicated, may hold values from -0.375 to 0.375
- w_key_absorb: bfloat16 [32, 64, 256], replicated, may hold values from -0.75 to 0.75
- latent_gain: bfloat16 [256], replicated, may hold values from 0.099609375 to 1.8984375
- w_latent_down: bfloat16 [2048, 256], replicated, may hold values from -0.125 to 0.125
- w_rotary_key: bfloat16 [2048, 32], replicated, may hold values from -0.125 to 0.125
- w_value_up: bfloat16 [32, 256, 64], replicated, may hold values from -0.375 to 0.375
- w_output: bfloat16 [2048, 2048], P(None, 'ep'), may hold values from -0.125 to 0.125
- ffn_gain: bfloat16 [2048], replicated, may hold values from 0.099609375 to 1.8984375
- expert_gate: bfloat16 [128, 2048, 512], P('ep'), may hold values from -0.125 to 0.125
- expert_up: bfloat16 [128, 2048, 512], P('ep'), may hold values from -0.125 to 0.125
- expert_down: bfloat16 [128, 512, 2048], P('ep'), may hold values from -0.25 to 0.25
- shared_gate: bfloat16 [2048, 256], replicated, may hold values from -0.125 to 0.125
- shared_up: bfloat16 [2048, 256], replicated, may hold values from -0.125 to 0.125
- shared_down: bfloat16 [256, 2048], replicated, may hold values from -0.375 to 0.375
Outputs:
- mixed: bfloat16 [3072, 2048], P('ep')
- latent_new: bfloat16 [3072, 256], P('ep')
- rotary_new: bfloat16 [3072, 32], P('ep')
Inputs may be any that keep to these rules, and one draw needn't show every extreme that they name: `route_ids`: within the rows of one device no expert is named by more than 3 rows, a bound that some block reaches; each row names 6 different experts. `lengths`: cache positions at or past a sequence's length are not read.
All inputs are finite; a program needn't handle non-finite values.
Results may differ from a plain program's by a relative error of at most 0.025.
Values may be sent and summed in bfloat16 or wider, within the bound.
No kernel may reach another device: no remote copies, remote signals or barrier semaphores. Data moves between devices by JAX's collectives and lax.ppermute only.
A program may use at most 128 MiB of HBM per device.

v0:
```python
import jax
import jax.numpy as jnp
from jax import lax
from jax.sharding import PartitionSpec as P

EPSILON = 1e-06
THETA = 10000.0
ROUTED_SCALE = 2.5


def rms_scale(values, gain):
    squares = jnp.mean(values * values, axis=-1, keepdims=True)
    return values * lax.rsqrt(squares + EPSILON) * gain.astype(jnp.float32)


def rotate(values, positions):
    half = values.shape[-1] // 2
    freqs = 1.0 / THETA ** (jnp.arange(half, dtype=jnp.float32) * 2.0 / values.shape[-1])
    angles = positions.astype(jnp.float32)[:, None] * freqs[None, :]
    if values.ndim == 3:
        angles = angles[:, None, :]
    cosine, sine = (jnp.cos(angles), jnp.sin(angles))
    first, second = (values[..., :half], values[..., half:])
    return jnp.concatenate(
        [first * cosine - second * sine, second * cosine + first * sine], axis=-1
    )


def shards(
    tokens,
    lengths,
    latent_cache,
    rotary_cache,
    route_ids,
    route_scores,
    attn_gain,
    w_query_down,
    query_gain,
    w_query_nope,
    w_query_rope,
    w_key_absorb,
    latent_gain,
    w_latent_down,
    w_rotary_key,
    w_value_up,
    w_output,
    ffn_gain,
    expert_gate,
    expert_up,
    expert_down,
    shared_gate,
    shared_up,
    shared_down,
):
    f32 = jnp.float32
    bf16 = jnp.bfloat16
    rows, model = tokens.shape
    heads, nope, latent = w_key_absorb.shape
    rotary = w_rotary_key.shape[1]
    top = route_ids.shape[1]
    normed = rms_scale(tokens.astype(f32), attn_gain).astype(bf16)
    query_low = rms_scale(
        jnp.dot(normed, w_query_down, preferred_element_type=f32), query_gain
    ).astype(bf16)
    query_nope = (
        jnp.dot(query_low, w_query_nope, preferred_element_type=f32)
        .astype(bf16)
        .reshape(rows, heads, nope)
    )
    query_rot = jnp.dot(query_low, w_query_rope, preferred_element_type=f32).reshape(
        rows, heads, rotary
    )
    query_rot = rotate(query_rot, lengths).astype(bf16)
    query_lat = jnp.einsum(
        "thn,hnl->thl", query_nope, w_key_absorb, preferred_element_type=f32
    ).astype(bf16)
    latent_new = rms_scale(
        jnp.dot(normed, w_latent_down, preferred_element_type=f32), latent_gain
    ).astype(bf16)
    rotary_new = rotate(jnp.dot(normed, w_rotary_key, preferred_element_type=f32), lengths).astype(
        bf16
    )
    scale = (nope + rotary) ** (-0.5)
    scores = (
        jnp.einsum("thl,tkl->thk", query_lat, latent_cache, preferred_element_type=f32)
        + jnp.einsum("thr,tkr->thk", query_rot, rotary_cache, preferred_element_type=f32)
    ) * scale
    live = jnp.arange(latent_cache.shape[1], dtype=jnp.int32)[None, :] < lengths[:, None]
    scores = jnp.where(live[:, None, :], scores, -jnp.inf)
    own = (
        jnp.einsum("thl,tl->th", query_lat, latent_new, preferred_element_type=f32)
        + jnp.einsum("thr,tr->th", query_rot, rotary_new, preferred_element_type=f32)
    ) * scale
    highest = jnp.maximum(jnp.max(scores, axis=-1), own)
    weights = jnp.exp(scores - highest[..., None])
    own_weight = jnp.exp(own - highest)
    total = jnp.sum(weights, axis=-1) + own_weight
    probs = (weights / total[..., None]).astype(bf16)
    own_prob = (own_weight / total).astype(bf16)
    out_lat = jnp.einsum("thk,tkl->thl", probs, latent_cache, preferred_element_type=f32)
    out_lat = (
        out_lat + own_prob.astype(f32)[..., None] * latent_new.astype(f32)[:, None, :]
    ).astype(bf16)
    values = jnp.einsum("thl,hlv->thv", out_lat, w_value_up, preferred_element_type=f32).astype(
        bf16
    )
    values = values.reshape(rows, model)
    attended = jnp.dot(
        values, lax.all_gather(w_output, "ep", axis=1, tiled=True), preferred_element_type=f32
    ).astype(bf16)
    residual = (tokens.astype(f32) + attended.astype(f32)).astype(bf16)
    ffn_in = rms_scale(residual.astype(f32), ffn_gain).astype(bf16)
    devices = lax.axis_size("ep")
    local_experts = expert_gate.shape[0]
    experts = devices * local_experts
    capacity = max(2, rows * top * 8 // (3 * experts))
    flat_ids = route_ids.reshape(-1)
    hits = (flat_ids[:, None] == jnp.arange(experts, dtype=jnp.int32)[None, :]).astype(jnp.int32)
    earlier = jnp.cumsum(hits, axis=0) - hits
    slot = jnp.sum(earlier * hits, axis=1)
    target = flat_ids * capacity + slot
    slot_range = jnp.arange(experts * capacity, dtype=jnp.int32)
    per_token = jnp.any(
        slot_range[:, None, None] == target.reshape(rows, top)[None, :, :], axis=2
    ).astype(bf16)
    per_pair = (target[:, None] == slot_range[None, :]).astype(bf16)
    outgoing = (
        jnp.dot(per_token, ffn_in, preferred_element_type=f32)
        .astype(bf16)
        .reshape(experts, capacity, model)
    )
    arrived = lax.all_to_all(outgoing, "ep", split_axis=0, concat_axis=0, tiled=True)
    count = arrived.shape[1]
    grouped = arrived.reshape(devices, local_experts, count, model)
    gate = jnp.einsum("sjcd,jdf->sjcf", grouped, expert_gate, preferred_element_type=f32)
    upward = jnp.einsum("sjcd,jdf->sjcf", grouped, expert_up, preferred_element_type=f32)
    hidden = (jax.nn.silu(gate) * upward).astype(bf16)
    result = jnp.einsum("sjcf,jfd->sjcd", hidden, expert_down, preferred_element_type=f32).astype(
        bf16
    )
    returned = lax.all_to_all(
        result.reshape(devices * local_experts, count, model),
        "ep",
        split_axis=0,
        concat_axis=0,
        tiled=True,
    )
    picked = jnp.dot(
        per_pair, returned.reshape(experts * capacity, model), preferred_element_type=f32
    )
    route_weight = ROUTED_SCALE * route_scores / jnp.sum(route_scores, axis=1, keepdims=True)
    routed = jnp.sum(picked.reshape(rows, top, model) * route_weight[:, :, None], axis=1)
    gate_shared = jnp.dot(ffn_in, shared_gate, preferred_element_type=f32)
    up_shared = jnp.dot(ffn_in, shared_up, preferred_element_type=f32)
    hidden_shared = (jax.nn.silu(gate_shared) * up_shared).astype(bf16)
    shared_out = jnp.dot(hidden_shared, shared_down, preferred_element_type=f32)
    mixed = (residual.astype(f32) + routed + shared_out).astype(bf16)
    return (mixed, latent_new, rotary_new)


def solution(mesh):
    return jax.shard_map(
        shards,
        mesh=mesh,
        in_specs=(
            P("ep", None),
            P("ep"),
            P("ep", None, None),
            P("ep", None, None),
            P("ep", None),
            P("ep", None),
            P(),
            P(),
            P(),
            P(),
            P(),
            P(),
            P(),
            P(),
            P(),
            P(),
            P(None, "ep"),
            P(),
            P("ep", None, None),
            P("ep", None, None),
            P("ep", None, None),
            P(),
            P(),
            P(),
        ),
        out_specs=(P("ep", None), P("ep", None), P("ep", None)),
        check_vma=False,
    )
```

profile of v0, /device:TPU:1, one launch (start us, length us, event | category | flops | bytes accessed | tf_op | source)
XLA Modules:
  0.0 198.8 jit_solution(13205841041242894401)
XLA Ops:
  9.3 1.0 fusion.55
  10.3 1.7 multiply_reduce_fusion.2
  12.0 1.3 fusion.79
  13.5 1.5 convolution_convert_fusion.2
  15.0 0.9 reshape.206
  16.4 1.6 multiply_reduce_fusion.1
  19.5 8.5 %fusion.50 = f32[24,32,1024]{2,1,0:T(8,128)S(1)} fusion(bf16[24,1024,256]{2,1,0:T(8,128)(2,1)} %param.26, bf16[24,32,256]{2,0,1:T(8,128)(2,1)S(1)} %fusion.32), kind=kOutput, calls=%fused_computation.50 | convolution fusion | flops 402653184 | bytes 16121856 | tf_op jit(solution)/shard_map/thl,tkl->thk/dot_general | solution.py:85
  28.0 2.6 %fusion.89 = (f32[24,32]{1,0:T(8,128)S(1)}, f32[24,32,1024]{2,1,0:T(8,128)S(1)}) fusion(f32[24,32,1024]{2,1,0:T(8,128)S(1)} %fusion.50, bf16[24,1024,32]{1,2,0:T(8,128)(2,1)} %param.27, bf16[24,32,16]{2,1,0:T(8,128)(2,1)S(1)} %get-tuple-element.6, bf16[24,32,16]{2,1,0:T(8,128)(2,1)S(1)} %get-tuple-element.5, pred[24,1024]{1,0:T(8,128)(4,1)S(1)} %iota_compare_fusion.2), kind=kOutput, calls=%fused_computation.118 | convolution fusion | flops 53574912 | bytes 7941120 | tf_op jit(solution)/shard_map/thr,tkr->thk/dot_general | solution.py:86
  31.3 2.1 %fusion.28 = bf16[24,32,256]{2,1,0:T(8,128)(2,1)S(1)} fusion(bf16[24,1024,256]{2,1,0:T(8,128)(2,1)S(1)} %bitcast.89, f32[24,32,1024]{2,1,0:T(8,128)S(1)} %get-tuple-element.16, f32[24,32]{1,0:T(8,128)S(1)} %get-tuple-element.8, f32[24,32]{1,0:T(8,128)S(1)} %fusion.74, f32[24,256]{1,0:T(8,128)S(1)} %get-tuple-element.3, f32[24,32]{1,0:T(8,128)S(1)} %get-tuple-element.7), kind=kOutput, calls=%fused_computation.30 | convolution fusion | flops 405602304 | bytes 16155648 | tf_op jit(solution)/shard_map/thk,tkl->thl/dot_general | solution.py:100
  35.2 49.1 %all-gather.2.cloned.1.call-done = bf16[2048,2048]{0,1:T(8,128)(2,1)} async-done(((bf16[2048,16]{0,1:T(8,128)(2,1)}), bf16[2048,2048]{0,1:T(8,128)(2,1)}) %all-gather.2.cloned.1.call-update) | async-done | bytes 8388624 | tf_op jit(solution)/shard_map/all_gather | solution.py:109
  84.3 5.8 %multiply_reduce_fusion = (f32[24]{0:T(128)S(1)}, f32[24,2048]{1,0:T(8,128)S(1)}) fusion(bf16[24,2048]{1,0:T(8,128)(2,1)S(1)} %reshape.208, bf16[2048,2048]{0,1:T(8,128)(2,1)} %all-gather.2.cloned.1.call-done, bf16[24,2048]{1,0:T(8,128)(2,1)S(1)} %copy-done.2), kind=kOutput, calls=%fused_computation.64 | convolution fusion | flops 201719776 | bytes 8781920 | tf_op jit(solution)/shard_map/dot_general | solution.py:108
  90.1 1.8 convolution_convert_fusion
  91.9 5.1 %reshape.211 = bf16[128,3,2048]{2,1,0:T(4,128)(2,1)} reshape(bf16[384,2048]{1,0:T(8,128)(2,1)} %convolution_convert_fusion) | data formatting | bytes 3145728 | tf_op jit(solution)/shard_map/reshape | solution.py:130
  97.1 35.8 %all_to_all.10 = bf16[128,3,2048]{2,1,0:T(4,128)(2,1)S(1)} all-to-all(bf16[128,3,2048]{2,1,0:T(4,128)(2,1)} %reshape.211), channel_id=1, replica_groups=mesh['ep'=128] {'ep'}, dimensions={0} | all-to-all | bytes 3145728 | tf_op jit(solution)/shard_map/all_to_all | solution.py:132
  132.9 1.3 copy-done.1
  134.3 1.9 fusion.14
  136.1 6.3 %convolution_convert_fusion.1 = bf16[128,3,2048]{2,0,1:T(8,128)(2,1)} fusion(bf16[1,512,2048]{2,1,0:T(8,128)(2,1)S(1)} %copy-done, bf16[1,2048,512]{2,1,0:T(8,128)(2,1)} %param.43, bf16[128,3,2048]{2,1,0:T(4,128)(2,1)} %copy-done.1, f32[128,1,3,512]{3,0,2,1:T(8,128)S(1)} %fusion.14), kind=kOutput, calls=%fused_computation.4 | convolution fusion | flops 1612578816 | bytes 8126464 | tf_op jit(solution)/shard_map/sjcf,jfd->sjcd/dot_general | solution.py:138
  142.4 4.1 %copy.78 = bf16[128,3,2048]{2,1,0:T(4,128)(2,1)} copy(bf16[128,3,2048]{2,0,1:T(8,128)(2,1)} %convolution_convert_fusion.1) | data formatting | bytes 3145728 | tf_op jit(solution)/shard_map/convert_element_type | solution.py:138
  146.5 5.6 %all-to-all-start.1 = ((bf16[128,3,2048]{2,1,0:T(4,128)(2,1)}), bf16[128,3,2048]{2,1,0:T(4,128)(2,1)}, u32[]{:S(2)}, u32[]{:S(2)}) async-start(bf16[128,3,2048]{2,1,0:T(4,128)(2,1)} %copy.78), calls=%async_computation.1 | async-start | bytes 4194304 | tf_op jit(solution)/shard_map/all_to_all | solution.py:141
  153.4 0.9 fusion.81
  154.3 28.0 %all-to-all-done.1 = bf16[128,3,2048]{2,1,0:T(4,128)(2,1)} async-done(((bf16[128,3,2048]{2,1,0:T(4,128)(2,1)}), bf16[128,3,2048]{2,1,0:T(4,128)(2,1)}, u32[]{:S(2)}, u32[]{:S(2)}) %all-to-all-start.1) | async-done | bytes 1572896 | tf_op jit(solution)/shard_map/all_to_all | solution.py:141
  182.3 5.1 %reshape.225 = bf16[384,2048,1]{1,0,2:T(8,128)(2,1)} reshape(bf16[128,3,2048]{2,1,0:T(4,128)(2,1)} %all-to-all-done.1) | data formatting | bytes 3145728 | tf_op jit(solution)/shard_map/reshape | solution.py:149
  187.4 1.9 fusion.24
  189.3 2.7 %fusion.1 = bf16[24,2048]{1,0:T(8,128)(2,1)} fusion(bf16[256,2048]{1,0:T(8,128)(2,1)S(1)} %copy-done.6, bf16[2048,256]{1,0:T(8,128)(2,1)} %param.46, f32[24,2048]{1,0:T(8,128)S(1)} %get-tuple-element.20, f32[24,2048]{1,0:T(8,128)S(1)} %fusion.24, f32[24,256]{1,0:T(8,128)} %fusion.81, f32[2048]{0:T(1024)S(1)} %convert_element_type.124, f32[24]{0:T(128)S(1)} %add_rsqrt_fusion), kind=kOutput, calls=%fused_computation.8 | convolution fusion | flops 50663424 | bytes 2621536 | tf_op jit(solution)/shard_map/dot_general | solution.py:156
  (85 shorter events, 7.9 us)
Async XLA Ops:
  7.2 129.0 %copy-start = (bf16[1,512,2048]{2,1,0:T(8,128)(2,1)S(1)}, bf16[1,512,2048]{2,1,0:T(8,128)(2,1)}, u32[]{:S(2)}) copy-start(bf16[1,512,2048]{2,1,0:T(8,128)(2,1)} %param.44) | copy-start | bytes 6291460
  7.2 8.7 %copy-start.2 = (bf16[24,2048]{1,0:T(8,128)(2,1)S(1)}, bf16[24,2048]{1,0:T(8,128)(2,1)}, u32[]{:S(2)}) copy-start(bf16[24,2048]{1,0:T(8,128)(2,1)} %param.24) | copy-start | bytes 294916
  7.2 6.3 %copy-start.12 = (s32[24]{0:T(128)S(1)}, s32[24]{0:T(128)}, u32[]{:S(2)}) copy-start(s32[24]{0:T(128)} %param.25) | copy-start | bytes 292
  7.2 8.7 %copy-start.15 = (bf16[256]{0:T(256)(128)(2,1)S(1)}, bf16[256]{0:T(256)(128)(2,1)}, u32[]{:S(2)}) copy-start(bf16[256]{0:T(256)(128)(2,1)} %param.36) | copy-start | bytes 1540
  7.2 8.7 %copy-start.14 = (bf16[2048,32]{0,1:T(8,128)(2,1)S(1)}, bf16[2048,32]{0,1:T(8,128)(2,1)}, u32[]{:S(2)}) copy-start(bf16[2048,32]{0,1:T(8,128)(2,1)} %param.38) | copy-start | bytes 393220
  7.2 77.1 %all-gather.2.cloned.1.call-start = ((), (), s32[]{:S(2)}) async-start(), calls=%async_computation.2 | async-start | bytes 8454144 | tf_op jit(solution)/shard_map/all_gather | solution.py:109
  15.9 2.8 %copy-start.3 = (bf16[32,64,256]{2,1,0:T(8,128)(2,1)S(1)}, bf16[32,64,256]{2,1,0:T(8,128)(2,1)}, u32[]{:S(2)}) copy-start(bf16[32,64,256]{2,1,0:T(8,128)(2,1)} %param.35) | copy-start | bytes 3145732
  15.9 2.8 %copy-start.7 = (bf16[24,32,64]{2,1,0:T(8,128)(2,1)S(1)}, bf16[24,32,64]{2,1,0:T(8,128)(2,1)}, u32[]{:S(2)}) copy-start(bf16[24,32,64]{2,1,0:T(8,128)(2,1)} %reshape.206) | copy-start | bytes 294916
  18.7 0.6 copy-start.10
  19.5 11.8 %slice-start = ((s8[12582912]{0:T(1024)(128)(4,1)}), s8[4194304]{0:T(1024)(128)(4,1)S(1)}, s32[]{:S(2)}) async-start(s8[12582912]{0:T(1024)(128)(4,1)} %bitcast.88), calls=%async_computation.3 | async-start | bytes 8388608
  19.5 11.8 %slice-start.1 = ((s8[12582912]{0:T(1024)(128)(4,1)}), s8[4194304]{0:T(1024)(128)(4,1)S(1)}, s32[]{:S(2)}) async-start(s8[12582912]{0:T(1024)(128)(4,1)} %bitcast.88), calls=%async_computation.4 | async-start | bytes 8388608
  28.0 3.3 %slice-start.2 = ((s8[12582912]{0:T(1024)(128)(4,1)}), s8[4194304]{0:T(1024)(128)(4,1)S(1)}, s32[]{:S(2)}) async-start(s8[12582912]{0:T(1024)(128)(4,1)} %bitcast.88), calls=%async_computation.5 | async-start | bytes 8388608
  31.3 2.1 %copy-start.4 = (bf16[32,256,64]{1,2,0:T(8,128)(2,1)S(1)}, bf16[32,256,64]{1,2,0:T(8,128)(2,1)}, u32[]{:S(2)}) copy-start(bf16[32,256,64]{1,2,0:T(8,128)(2,1)} %param.39) | copy-start | bytes 3145732
  33.4 0.8 copy-start.9
  33.4 1.7 copy-start.11
  97.1 37.2 %copy-start.13 = (bf16[1,2048,512]{2,1,0:T(8,128)(2,1)S(1)}, bf16[1,2048,512]{2,1,0:T(8,128)(2,1)}, u32[]{:S(2)}) copy-start(bf16[1,2048,512]{2,1,0:T(8,128)(2,1)} %param.42) | copy-start | bytes 6291460
  132.9 1.4 copy-start.1
  146.5 5.6 %copy-start.8 = (f32[24,6]{0,1:T(8,128)S(1)}, f32[24,6]{0,1:T(8,128)}, u32[]{:S(2)}) copy-start(f32[24,6]{0,1:T(8,128)} %param.29) | copy-start | bytes 1732
  146.5 6.9 %copy-start.5 = (bf16[2048,256]{1,0:T(8,128)(2,1)S(1)}, bf16[2048,256]{1,0:T(8,128)(2,1)}, u32[]{:S(2)}) copy-start(bf16[2048,256]{1,0:T(8,128)(2,1)} %param.45) | copy-start | bytes 3145732
  146.5 35.8 %all-to-all-start.1 = ((bf16[128,3,2048]{2,1,0:T(4,128)(2,1)}), bf16[128,3,2048]{2,1,0:T(4,128)(2,1)}, u32[]{:S(2)}, u32[]{:S(2)}) async-start(bf16[128,3,2048]{2,1,0:T(4,128)(2,1)} %copy.78), calls=%async_computation.1 | async-start | bytes 4194304 | tf_op jit(solution)/shard_map/all_to_all | solution.py:141
  154.3 35.1 %copy-start.6 = (bf16[256,2048]{1,0:T(8,128)(2,1)S(1)}, bf16[256,2048]{1,0:T(8,128)(2,1)}, u32[]{:S(2)}) copy-start(bf16[256,2048]{1,0:T(8,128)(2,1)} %param.47) | copy-start | bytes 3145732
Sparse Core Ops, SparseCore 0:
  11.0 73.2 all-gather.1
where the time goes:
time: 200 us; the launch traced here: 199 us
  waiting for transfers between devices  77.8 us (39%)
  matrix products  41.9 us (21%)
  blocking collectives  35.8 us (18%)
  local copies, waits for them, and re-layouts  17.7 us (9%)
  between operations  14.4 us (7%)
  starting transfers between devices  5.63 us (3%)
  other arithmetic  5.58 us (3%)
    all_gather x1, waiting for transfers between devices, shards(): lax.all_gather(w_output, 'ep', axis=1, tiled=True)  49.1 us
    all_to_all x1, blocking collectives, shards(): lax.all_to_all(outgoing, 'ep', split_axis=0, concat_axis=0, tiled=True)  35.8 us
    all_to_all x1, waiting for transfers between devices, shards(): lax.all_to_all(result.reshape(devices * local_experts, count, model), 'ep...  28 us
    dot_general x1, matrix products, shards(): jnp.einsum('thl,tkl->thk', query_lat, latent_cache, preferred_element_typ...  8.48 us
    dot_general x1, matrix products, shards(): jnp.einsum('sjcf,jfd->sjcd', hidden, expert_down, preferred_element_type=...  6.27 us
    dot_general x1, matrix products, shards(): jnp.dot(values, lax.all_gather(w_output, 'ep', axis=1, tiled=True), prefe...  5.77 us
    all_to_all x1, starting transfers between devices, shards(): lax.all_to_all(result.reshape(devices * local_experts, count, model), 'ep...  5.59 us
    reshape x1, local copies, waits for them, and re-layouts, shards(): outgoing = jnp.dot(per_token, ffn_in, preferred_element_type=f32).astype(...  5.15 us
  transfers between devices with their start and end apart: 2, of which 2 were waited for; matrix products, arithmetic and copies ran while one was open for 15% of the time, Pallas kernels for 0%

commit v1 on v0

v1 whole, which is shorter than its diff:
```python
import functools

import jax
import jax.numpy as jnp
from jax import lax
from jax.experimental import pallas as pl
from jax.experimental.pallas import tpu as pltpu
from jax.sharding import Mesh
from jax.sharding import PartitionSpec as P

EPSILON = 1e-06
THETA = 10000.0
ROUTED_SCALE = 2.5
f32 = jnp.float32
bf16 = jnp.bfloat16

NT = (((1,), (1,)), ((), ()))
NN = (((1,), (0,)), ((), ()))
SEQ_STEP = 4


def dot(a, b, dims=NN):
    return lax.dot_general(a, b, dims, preferred_element_type=f32)


def rms(values, gain):
    squares = jnp.mean(values * values, axis=-1, keepdims=True)
    return values * lax.rsqrt(squares + EPSILON) * gain


def turn(tile, cosine, sine):
    lane = lax.broadcasted_iota(jnp.int32, tile.shape, 1)
    swapped = jnp.where(lane % 32 < 16, pltpu.roll(tile, 112, 1), pltpu.roll(tile, 16, 1))
    return tile * cosine + swapped * sine


def attend_kernel(
    lengths,
    tokens,
    cosine,
    sine,
    latent,
    rotary,
    attn_gain,
    w_qd,
    q_gain,
    w_qn,
    w_qr,
    w_ka,
    l_gain,
    w_ld,
    w_rk,
    w_vu,
    values,
    latent_new,
    rotary_new,
    q_lat,
    q_rot,
    o_lat,
    l_new,
    r_new,
):
    step = pl.program_id(0)
    rows = tokens.shape[0]
    heads = w_ka.shape[0]
    lat = w_qd.shape[1]
    scale = (w_ka.shape[1] + w_rk.shape[0]) ** (-0.5)

    @pl.when(step == 0)
    def _():
        normed = rms(tokens[...].astype(f32), attn_gain[...].astype(f32)).astype(bf16)
        low = rms(dot(normed, w_qd[...]), q_gain[...].astype(f32)).astype(bf16)
        fresh = rms(dot(normed, w_ld[...]), l_gain[...].astype(f32)).astype(bf16)
        latent_new[...] = fresh
        l_new[...] = fresh.astype(f32)
        cos, sin = cosine[...], sine[...]
        w_four = jnp.concatenate([w_rk[...]] * 4, axis=0)
        turned = turn(dot(normed, w_four, NT), cos, sin).astype(bf16)
        rotary_new[...] = turned[:, :32]
        r_new[...] = turned.astype(f32)
        nope = dot(low, w_qn[...]).astype(bf16)
        for h in range(heads):
            part = dot(nope[:, h * 64 : h * 64 + 64], w_ka[h])
            for c in range(lat // 128):
                q_lat[c, pl.ds(h, rows, stride=heads), :] = part[:, c * 128 : c * 128 + 128]
        rope = dot(low, w_qr[...])
        for j in range(heads // 4):
            tile = turn(rope[:, j * 128 : j * 128 + 128], cos, sin)
            for q in range(4):
                shifted = tile if q == 0 else pltpu.roll(tile, 128 - 32 * q, 1)
                q_rot[pl.ds(4 * j + q, rows, stride=heads), :] = shifted

    cache = latent.shape[1]
    first = step * SEQ_STEP
    base = pl.multiple_of(first * heads, SEQ_STEP * heads)
    span = SEQ_STEP * heads
    q_all = jnp.concatenate(
        [q_lat[c, pl.ds(base, span), :] for c in range(lat // 128)], axis=1
    ).astype(bf16)
    owner = lax.broadcasted_iota(jnp.int32, (span, lat), 0) // heads
    group = lax.broadcasted_iota(jnp.int32, (heads, 128), 1) // 32
    lane = lax.broadcasted_iota(jnp.int32, (1, 128), 1) // 32
    rot_rows = []
    news = []
    new_rot = jnp.zeros((1, 128), f32)
    limit = jnp.zeros((1, 128), jnp.int32)
    scores = None
    own = None
    for j in range(SEQ_STEP):
        part = q_rot[pl.ds(base + j * heads, heads), :]
        part = part if j == 0 else pltpu.roll(part, 32 * j, 1)
        rot_rows.append(jnp.where(group == j, part, 0.0))
        new_rot = jnp.where(lane == j, r_new[pl.ds(first + j, 1), :], new_rot)
        limit = jnp.where(lane == j, lengths[first + j], limit)
        news.append(l_new[pl.ds(first + j, 1), :])
        q_j = jnp.where(owner == j, q_all, jnp.zeros_like(q_all))
        s_j = dot(latent[j], q_j, NT)
        o_j = dot(jnp.broadcast_to(news[j], (8, lat)).astype(bf16), q_j, NT)
        scores = s_j if j == 0 else scores + s_j
        own = o_j if j == 0 else own + o_j
    rot_q = jnp.concatenate(rot_rows, axis=0).astype(bf16)
    rot_keys = rotary[...].reshape(SEQ_STEP * 32, cache)
    scores = (scores + dot(rot_q, rot_keys).T) * scale
    own = (own + dot(jnp.broadcast_to(new_rot, (8, 128)).astype(bf16), rot_q, NT)) * scale
    own = own[:1]
    place = lax.broadcasted_iota(jnp.int32, scores.shape, 0)
    scores = jnp.where(place < limit, scores, -jnp.inf)
    top = jnp.maximum(jnp.max(scores, axis=0, keepdims=True), own)
    weights = jnp.exp(scores - top)
    own_weight = jnp.exp(own - top)
    inverse = 1.0 / (jnp.sum(weights, axis=0, keepdims=True) + own_weight)
    probs = (weights * inverse).T.astype(bf16)
    own_prob = jnp.broadcast_to((own_weight * inverse).astype(bf16).astype(f32), (8, 128)).T
    for j in range(SEQ_STEP):
        sl = slice(j * heads, (j + 1) * heads)
        out = dot(probs[sl], latent[j]) + own_prob[sl, :1] * news[j]
        for c in range(lat // 128):
            o_lat[c, pl.ds(base + j * heads, heads), :] = out[:, c * 128 : c * 128 + 128]

    @pl.when(step == pl.num_programs(0) - 1)
    def _():
        for g in range(heads // 2):
            pair = []
            for h in (2 * g, 2 * g + 1):
                rows_h = jnp.concatenate(
                    [o_lat[c, pl.ds(h, rows, stride=heads), :] for c in range(lat // 128)], axis=1
                ).astype(bf16)
                pair.append(dot(rows_h, w_vu[h], NT))
            values[:, g * 128 : g * 128 + 128] = jnp.concatenate(pair, axis=1).astype(bf16)


def whole(shape):
    zeros = (0,) * len(shape)
    return pl.BlockSpec(shape, lambda *_: zeros)


def smem():
    return pl.BlockSpec(memory_space=pltpu.SMEM)


def vmem():
    return pl.BlockSpec(memory_space=pltpu.VMEM)


def room(mib):
    return pltpu.CompilerParams(vmem_limit_bytes=mib * 2**20)


def near_core(*arrays):
    return [pltpu.with_memory_space_constraint(a, pltpu.VMEM) for a in arrays]


def attend(lengths, tokens, cosine, sine, latent, rotary, *weights):
    rows, model = tokens.shape
    cache, lat = latent.shape[1:]
    rope = rotary.shape[1]
    heads = weights[5].shape[0]
    return pl.pallas_call(
        attend_kernel,
        grid=(rows // SEQ_STEP,),
        in_specs=[
            smem(),
            whole(tokens.shape),
            whole(cosine.shape),
            whole(sine.shape),
            pl.BlockSpec((SEQ_STEP, cache, lat), lambda i: (i, 0, 0)),
            pl.BlockSpec((SEQ_STEP, rope, cache), lambda i: (i, 0, 0)),
            *[whole(w.shape) for w in weights],
        ],
        out_specs=[whole((rows, model)), whole((rows, lat)), whole((rows, rope))],
        out_shape=[
            jax.ShapeDtypeStruct((rows, model), bf16),
            jax.ShapeDtypeStruct((rows, lat), bf16),
            jax.ShapeDtypeStruct((rows, rope), bf16),
        ],
        scratch_shapes=[
            pltpu.VMEM((lat // 128, rows * heads, 128), f32),
            pltpu.VMEM((rows * heads, 128), f32),
            pltpu.VMEM((lat // 128, rows * heads, 128), f32),
            pltpu.VMEM((rows, lat), f32),
            pltpu.VMEM((rows, 128), f32),
        ],
        cost_estimate=pl.CostEstimate(
            flops=4 * 10**9, bytes_accessed=22 * 10**6, transcendentals=10**6
        ),
        compiler_params=room(32),
        name="attend",
    )(
        lengths,
        tokens,
        cosine,
        sine,
        *[pltpu.with_memory_space_constraint(a, pltpu.HBM) for a in (latent, rotary, *weights)],
    )


def project_kernel(side, mine, other, v0, v1, v2, out, w):
    c = side[0]
    w[:, c] = mine[...]
    w[:, 1 - c] = other[...]
    columns = w[...].reshape(w.shape[0] * 2 * w.shape[2], w.shape[3])
    vals = jnp.concatenate([v0[...], v1[...], v2[...]], axis=0)
    out[...] = dot(vals, columns, NT).astype(bf16)


def project(side, mine, other, v0, v1, v2):
    groups, cols, model = mine.shape
    rows = v0.shape[0] + v1.shape[0] + v2.shape[0]
    return pl.pallas_call(
        project_kernel,
        in_specs=[smem()] + [vmem()] * 5,
        out_specs=vmem(),
        out_shape=pltpu.VMEM((rows, groups * 2 * cols), bf16),
        scratch_shapes=[pltpu.VMEM((groups, 2, cols, model), bf16)],
        compiler_params=room(12),
        name="project",
    )(side, *near_core(mine, other, v0, v1, v2))


def dispatch_kernel(place, target, here, far, near, tokens, gain, out, residual, ffn, blocks, tiles):
    z = place[0]
    rows = tokens.shape[0]
    blocks[z] = here[:rows]
    blocks[3 - z] = far[:rows]
    blocks[z ^ 1] = near[0]
    blocks[(3 - z) ^ 1] = near[1]
    attended = jnp.concatenate([blocks[b] for b in range(4)], axis=1)
    total = (tokens[...].astype(f32) + attended.astype(f32)).astype(bf16)
    residual[...] = total
    normed = rms(total.astype(f32), gain[...].astype(f32))
    ffn[...] = normed.astype(bf16)
    for c in range(16):
        tiles[pl.ds(c, rows, stride=16), :] = normed[:, c * 128 : c * 128 + 128]
    out[...] = jnp.zeros_like(out)

    def send(t, _):
        tile = tiles[pl.ds(pl.multiple_of(t * 16, 16), 16), :].astype(bf16)
        for k in range(6):
            out[target[t * 6 + k]] = tile
        return _

    lax.fori_loop(0, rows, send, 0, unroll=4)


def dispatch(place, target, here, far, near, tokens, gain, slots):
    rows, model = tokens.shape
    return pl.pallas_call(
        dispatch_kernel,
        in_specs=[smem(), smem()] + [vmem()] * 5,
        out_specs=[vmem()] * 3,
        out_shape=[
            pltpu.VMEM((slots, 16, 128), bf16),
            pltpu.VMEM((rows, model), bf16),
            pltpu.VMEM((rows, model), bf16),
        ],
        scratch_shapes=[
            pltpu.VMEM((4, rows, model // 4), bf16),
            pltpu.VMEM((rows * 16, 128), f32),
        ],
        compiler_params=room(10),
        name="dispatch",
    )(place, target, *near_core(here, far, near, tokens, gain))


def shared_kernel(residual, ffn, gate, up, down, out):
    g = dot(ffn[...], gate[...])
    hidden = (g * jax.nn.sigmoid(g) * dot(ffn[...], up[...])).astype(bf16)
    out[...] = residual[...].astype(f32) + dot(hidden, down[...])


def shared(residual, ffn, gate, up, down):
    args = (residual, ffn, gate, up, down)
    return pl.pallas_call(
        shared_kernel,
        in_specs=[vmem()] * 5,
        out_specs=vmem(),
        out_shape=pltpu.VMEM(residual.shape, f32),
        cost_estimate=pl.CostEstimate(
            flops=10**9, bytes_accessed=4 * 10**6, transcendentals=10**4
        ),
        compiler_params=room(10),
        name="shared",
    )(*near_core(*args))


def expert_kernel(arrived, gate, up, down, out, wide, x):
    peers, depth, lanes = arrived.shape
    slots = depth // 16
    wide[...] = arrived[...].astype(f32).reshape(peers * depth, lanes)
    for s in range(slots):
        for c in range(16):
            rows = wide[pl.ds(s * 16 + c, peers, stride=depth), :]
            x[s * peers : (s + 1) * peers, c * 128 : c * 128 + 128] = rows.astype(bf16)
    g = dot(x[...], gate[0])
    hidden = (g * jax.nn.sigmoid(g) * dot(x[...], up[0])).astype(bf16)
    result = dot(hidden, down[0])
    for s in range(slots):
        for c in range(16):
            wide[pl.ds(s * 16 + c, peers, stride=depth), :] = result[
                s * peers : (s + 1) * peers, c * 128 : c * 128 + 128
            ]
    out[...] = wide[...].reshape(peers, depth, lanes).astype(bf16)


def experts(arrived, gate, up, down):
    peers, depth, lanes = arrived.shape
    return pl.pallas_call(
        expert_kernel,
        in_specs=[vmem()] * 4,
        out_specs=vmem(),
        out_shape=pltpu.VMEM(arrived.shape, bf16),
        scratch_shapes=[
            pltpu.VMEM((peers * depth, lanes), f32),
            pltpu.VMEM((peers * depth // 16, 2048), bf16),
        ],
        compiler_params=room(28),
        name="experts",
    )(*near_core(arrived, gate, up, down))


def combine_kernel(target, weight, returned, base, out, tiles):
    rows = base.shape[0]

    def gather(t, _):
        total = jnp.zeros((16, 128), f32)
        for k in range(6):
            p = t * 6 + k
            total = total + returned[target[p]].astype(f32) * weight[p]
        tiles[pl.ds(pl.multiple_of(t * 16, 16), 16), :] = total
        return _

    lax.fori_loop(0, rows, gather, 0, unroll=4)
    for c in range(16):
        sl = slice(c * 128, c * 128 + 128)
        out[:, sl] = (base[:, sl] + tiles[pl.ds(c, rows, stride=16), :]).astype(bf16)


def combine(target, weight, returned, base):
    rows = base.shape[0]
    return pl.pallas_call(
        combine_kernel,
        in_specs=[smem(), smem(), vmem(), vmem()],
        out_specs=vmem(),
        out_shape=pltpu.VMEM(base.shape, bf16),
        scratch_shapes=[pltpu.VMEM((rows * 16, 128), f32)],
        compiler_params=room(8),
        name="combine",
    )(target, weight, *near_core(returned, base))


def shards(
    tokens,
    lengths,
    latent_cache,
    rotary_cache,
    route_ids,
    route_scores,
    attn_gain,
    w_query_down,
    query_gain,
    w_query_nope,
    w_query_rope,
    w_key_absorb,
    latent_gain,
    w_latent_down,
    w_rotary_key,
    w_value_up,
    w_output,
    ffn_gain,
    expert_gate,
    expert_up,
    expert_down,
    shared_gate,
    shared_up,
    shared_down,
):
    rows, model = tokens.shape
    rotary = w_rotary_key.shape[1]
    top = route_ids.shape[1]
    devices = 128
    capacity = 3
    everyone = ("z", "y", "x", "c")
    z, c = lax.axis_index("z"), lax.axis_index("c")

    columns = w_output.T
    sent = jnp.broadcast_to(columns[None], (16,) + columns.shape)
    mine = lax.all_to_all(sent, ("y", "x"), 0, 0, tiled=True)

    half = rotary // 2
    freqs = 1.0 / THETA ** (jnp.arange(half, dtype=f32) * 2.0 / rotary)
    angles = lengths.astype(f32)[:, None] * jnp.tile(freqs, 8)[None, :]
    sign = jnp.where(jnp.arange(128) % rotary < half, -1.0, 1.0)
    cosine, sine = jnp.cos(angles), jnp.sin(angles) * sign[None, :]

    values, latent_new, rotary_new = attend(
        lengths,
        tokens,
        cosine,
        sine,
        latent_cache,
        rotary_cache.transpose(0, 2, 1),
        attn_gain[None],
        w_query_down,
        query_gain[None],
        w_query_nope,
        w_query_rope,
        w_key_absorb,
        latent_gain[None],
        w_latent_down,
        w_rotary_key.T,
        w_value_up.transpose(0, 2, 1),
    )

    same = route_ids[:, None, :, None] == route_ids[None, :, None, :]
    before = jnp.arange(rows)[None, :] < jnp.arange(rows)[:, None]
    slot = jnp.sum((same & before[:, :, None, None]).astype(jnp.int32), axis=(1, 3))
    target = (route_ids * capacity + slot).reshape(-1)
    weight = ROUTED_SCALE * route_scores / jnp.sum(route_scores, axis=1, keepdims=True)

    mine, values = lax.optimization_barrier((mine, values))
    other = lax.ppermute(mine, "c", [(0, 1), (1, 0)])
    pair = [(0, 1), (1, 0), (2, 3), (3, 2)]
    cross = [(0, 3), (3, 0), (1, 2), (2, 1)]
    v1 = lax.ppermute(values, "z", pair)
    both = jnp.concatenate([values, v1], axis=0)
    v2 = lax.ppermute(both, "z", cross)
    here = project(c.reshape(1), mine, other, values, v1, v2)
    far = lax.ppermute(here[2 * rows :], "z", cross)
    near = lax.ppermute(
        jnp.stack([here[rows : 2 * rows], far[rows:]], axis=0), "z", pair
    )
    out, residual, ffn = dispatch(
        z.reshape(1), target, here, far, near, tokens, ffn_gain[None], devices * capacity
    )
    arrived = lax.all_to_all(
        out.reshape(devices, capacity * 16, 128), everyone, 0, 0, tiled=True
    )
    base = shared(residual, ffn, shared_gate, shared_up, shared_down)
    result = experts(arrived, expert_gate, expert_up, expert_down)
    returned = lax.all_to_all(result, everyone, 0, 0, tiled=True)
    mixed = combine(
        target, weight.reshape(-1), returned.reshape(devices * capacity, 16, 128), base
    )
    return (mixed, latent_new, rotary_new)


def solution(mesh):
    grid = Mesh(mesh.devices.reshape(4, 4, 4, 2), ("z", "y", "x", "c"))
    ep = ("z", "y", "x", "c")
    return jax.shard_map(
        shards,
        mesh=grid,
        in_specs=(
            P(ep, None),
            P(ep),
            P(ep, None, None),
            P(ep, None, None),
            P(ep, None),
            P(ep, None),
            P(),
            P(),
            P(),
            P(),
            P(),
            P(),
            P(),
            P(),
            P(),
            P(),
            P(None, ep),
            P(),
            P(ep, None, None),
            P(ep, None, None),
            P(ep, None, None),
            P(),
            P(),
            P(),
        ),
        out_specs=(P(ep, None), P(ep, None), P(ep, None)),
        check_vma=False,
    )
```

time: 200 us -> 130 us (0.65)
  waiting for transfers between devices: 77.8 us -> 33.1 us
  matrix products: 41.9 us -> 0 us
  Pallas kernels: 0 us -> 25.2 us
  starting transfers between devices: 5.63 us -> 20.8 us
  between operations: 14.4 us -> 0.88 us
  local copies, waits for them, and re-layouts: 17.7 us -> 11.2 us
  other arithmetic: 5.58 us -> 0.47 us
    all_gather x1 -> x0, waiting for transfers between devices: 49.1 us -> none  [shards(): lax.all_gather(w_output, 'ep', axis=1, tiled=True)]
    dot_general x19 -> x0, matrix products: 41.9 us -> none  [the longest x1 8.48 us: shards(): jnp.einsum('thl,tkl->thk', query_lat, latent_cache, preferred_element_typ...]
    pallas_call x0 -> x6, Pallas kernels: none -> 25.2 us  [the longest x1 16.4 us: attend(): pl.pallas_call(attend_kernel, grid=(rows // SEQ_STEP,), in_specs=[smem(),...]
    ppermute x0 -> x5, waiting for transfers between devices: none -> 11.5 us  [the longest x1 4.05 us: shards(): v2 = lax.ppermute(both, 'z', cross)]
    reshape x5 -> x2, local copies, waits for them, and re-layouts: 11.5 us -> 0.19 us  [the longest x1 0.1 us: shards(): weight.reshape(-1)]
    ppermute x0 -> x5, starting transfers between devices: none -> 8.71 us  [the longest x1 3.48 us: shards(): v2 = lax.ppermute(both, 'z', cross)]
    all_to_all x1 -> x2, starting transfers between devices: 5.59 us -> 12.1 us  [the longest x1 7.57 us: shards(): mine = lax.all_to_all(sent, ('y', 'x'), 0, 0, tiled=True)]
    all_to_all x1 -> x2, waiting for transfers between devices: 28 us -> 21.6 us  [the longest x1 21.6 us: shards(): returned = lax.all_to_all(result, everyone, 0, 0, tiled=True)]
  transfers between devices with their start and end apart: 2 -> 7, of which waited for: 2 -> 5; matrix products, arithmetic and copies ran while one was open for 15% -> 2% of each run, Pallas kernels for 0% -> 13%
where the time goes in v1:
time: 130 us; the launch traced here: 129 us
  blocking collectives  37.6 us (29%)
  waiting for transfers between devices  33.1 us (25%)
  Pallas kernels  25.2 us (19%)
  starting transfers between devices  20.8 us (16%)
  local copies, waits for them, and re-layouts  11.2 us (9%)
    all_to_all x1, blocking collectives, shards(): lax.all_to_all(out.reshape(devices, capacity * 16, 128), everyone, 0, 0,...  37.6 us
    all_to_all x1, waiting for transfers between devices, shards(): returned = lax.all_to_all(result, everyone, 0, 0, tiled=True)  21.6 us
    pallas_call x1, Pallas kernels, attend(): pl.pallas_call(attend_kernel, grid=(rows // SEQ_STEP,), in_specs=[smem(),...  16.4 us
    all_to_all x1, starting transfers between devices, shards(): mine = lax.all_to_all(sent, ('y', 'x'), 0, 0, tiled=True)  7.57 us
    unnamed x33, local copies, waits for them, and re-layouts  6.96 us
    pallas_call x1, Pallas kernels, experts(): pl.pallas_call(expert_kernel, in_specs=[vmem()] * 4, out_specs=vmem(), ou...  5.24 us
    all_to_all x1, starting transfers between devices, shards(): returned = lax.all_to_all(result, everyone, 0, 0, tiled=True)  4.53 us
    ppermute x1, waiting for transfers between devices, shards(): v2 = lax.ppermute(both, 'z', cross)  4.05 us
  transfers between devices with their start and end apart: 7, of which 5 were waited for; matrix products, arithmetic and copies ran while one was open for 2% of the time, Pallas kernels for 13%

profile of v1, /device:TPU:1, one launch (start us, length us, event | category | flops | bytes accessed | tf_op | source)
XLA Modules:
  0.0 129.2 jit_solution(13178803333041216136)
XLA Ops:
  0.7 2.0 %broadcast_in_dim.18 = bf16[16,16,2048]{2,1,0:T(8,128)(2,1)} broadcast(bf16[16,2048]{1,0:T(8,128)(2,1)} %bitcast.17), dimensions={1,2} | broadcast | bytes 1114112 | tf_op jit(solution)/shard_map/broadcast_in_dim | solution.py:406
  2.7 7.6 %all-to-all-start = ((bf16[16,16,2048]{2,1,0:T(8,128)(2,1)}), bf16[16,16,2048]{2,1,0:T(8,128)(2,1)S(1)}, u32[]{:S(2)}, u32[]{:S(2)}) async-start(bf16[16,16,2048]{2,1,0:T(8,128)(2,1)} %broadcast_in_dim.18), calls=%async_computation | async-start | bytes 2097152 | tf_op jit(solution)/shard_map/all_to_all | solution.py:407
  12.3 16.4 %attend.1 = (bf16[24,2048]{1,0:T(8,128)(2,1)S(1)}, bf16[24,256]{1,0:T(8,128)(2,1)}, bf16[24,32]{1,0:T(8,128)(2,1)}) custom-call(s32[24]{0:T(128)S(1)} %copy-done.6, bf16[24,2048]{1,0:T(8,128)(2,1)S(1)} %copy-done.5, f32[24,128]{1,0:T(8,128)S(1)} %get-tuple-element.20.cosine, f32[24,128]{1,0:T(8,128)S(1)} %get-tuple-element.19.sine, ...), custom_call_target="tpu_custom_call" | custom-call | flops 4000000000 | bytes 22000000 | tf_op jit(solution)/shard_map/attend/pallas_call | solution.py:178
  28.7 1.0 collective-permute-start
  29.7 1.6 %collective-permute-start.1 = (bf16[24,2048]{1,0:T(8,128)(2,1)S(1)}, bf16[24,2048]{1,0:T(8,128)(2,1)S(1)}, u32[]{:S(2)}, u32[]{:S(2)}) collective-permute-start(bf16[24,2048]{1,0:T(8,128)(2,1)S(1)} %get-tuple-element.13.v0), channel_id=1, source_target_pairs={{0,32},{32,0},{64,96},{96,64},{1,33},{33,1},{65,97},{97,65},{2,34}... | collective-permute-start | bytes 294920 | tf_op jit(solution)/shard_map/ppermute | solution.py:444
  31.4 3.0 %collective-permute-done.1.v1 = bf16[24,2048]{1,0:T(8,128)(2,1)S(1)} collective-permute-done((bf16[24,2048]{1,0:T(8,128)(2,1)S(1)}, bf16[24,2048]{1,0:T(8,128)(2,1)S(1)}, u32[]{:S(2)}, u32[]{:S(2)}) %collective-permute-start.1) | collective-permute-done | bytes 98336 | tf_op jit(solution)/shard_map/ppermute | solution.py:444
  34.4 3.5 %collective-permute-start.2 = (bf16[48,2048]{1,0:T(8,128)(2,1)S(1)}, bf16[48,2048]{1,0:T(8,128)(2,1)S(1)}, u32[]{:S(2)}, u32[]{:S(2)}) collective-permute-start(bf16[48,2048]{1,0:T(8,128)(2,1)S(1)} %pad_maximum_fusion), channel_id=1, source_target_pairs={{0,96},{96,0},{32,64},{64,32},{1,97},{97,1},{33,65},{65,33},{2,98}... | collective-permute-start | bytes 589832 | tf_op jit(solution)/shard_map/ppermute | solution.py:446
  38.1 4.1 %collective-permute-done.2.v2 = bf16[48,2048]{1,0:T(8,128)(2,1)S(1)} collective-permute-done((bf16[48,2048]{1,0:T(8,128)(2,1)S(1)}, bf16[48,2048]{1,0:T(8,128)(2,1)S(1)}, u32[]{:S(2)}, u32[]{:S(2)}) %collective-permute-start.2) | collective-permute-done | bytes 196640 | tf_op jit(solution)/shard_map/ppermute | solution.py:446
  42.2 1.0 copy-done.3
  43.2 1.2 copy-done.4
  44.4 0.9 project.1.here
  45.4 2.5 %collective-permute-start.3 = (bf16[48,512]{1,0:T(8,128)(2,1)S(1)}, bf16[48,512]{1,0:T(8,128)(2,1)S(1)}, u32[]{:S(2)}, u32[]{:S(2)}) collective-permute-start(bf16[48,512]{1,0:T(8,128)(2,1)S(1)} %slice.12), channel_id=1, source_target_pairs={{0,96},{96,0},{32,64},{64,32},{1,97},{97,1},{33,65},{65,33},{2,98}... | collective-permute-start | bytes 147464 | tf_op jit(solution)/shard_map/ppermute | solution.py:448
  47.8 1.8 %collective-permute-done.3.far = bf16[48,512]{1,0:T(8,128)(2,1)S(1)} collective-permute-done((bf16[48,512]{1,0:T(8,128)(2,1)S(1)}, bf16[48,512]{1,0:T(8,128)(2,1)S(1)}, u32[]{:S(2)}, u32[]{:S(2)}) %collective-permute-start.3) | collective-permute-done | bytes 49184 | tf_op jit(solution)/shard_map/ppermute | solution.py:448
  49.9 2.7 %collective-permute-done.4.near = bf16[2,24,512]{2,1,0:T(8,128)(2,1)S(1)} collective-permute-done((bf16[2,24,512]{2,1,0:T(8,128)(2,1)S(1)}, bf16[2,24,512]{2,1,0:T(8,128)(2,1)S(1)}, u32[]{:S(2)}, u32[]{:S(2)}) %collective-permute-start.4) | collective-permute-done | bytes 49184 | tf_op jit(solution)/shard_map/ppermute | solution.py:449
  52.6 1.1 dispatch.1
  53.7 37.6 %all_to_all.15.arrived = bf16[128,48,128]{2,1,0:T(8,128)(2,1)S(1)} all-to-all(bf16[128,48,128]{2,1,0:T(8,128)(2,1)S(1)} %bitcast.13), channel_id=1, replica_groups=mesh['z'=4,'y'=4,'x'=4,'c'=2] {'z','y','x','c'}, dimensions={0} | all-to-all | bytes 3145728 | tf_op jit(solution)/shard_map/all_to_all | solution.py:455
  91.3 1.6 %copy-done.2 = bf16[1,512,2048]{2,1,0:T(8,128)(2,1)S(1)} copy-done((bf16[1,512,2048]{2,1,0:T(8,128)(2,1)S(1)}, bf16[1,512,2048]{2,1,0:T(8,128)(2,1)}, u32[]{:S(2)}) %copy-start.2) | copy-done | bytes 2097176
  92.9 5.2 %experts.1 = bf16[128,48,128]{2,1,0:T(8,128)(2,1)} custom-call(bf16[128,48,128]{2,1,0:T(8,128)(2,1)S(1)} %all_to_all.15.arrived, bf16[1,2048,512]{2,1,0:T(8,128)(2,1)S(1)} %copy-done, bf16[1,2048,512]{2,1,0:T(8,128)(2,1)S(1)} %copy-done.1, bf16[1,512,2048]{2,1,0:T(8,128)(2,1)S(1)} %copy-done.2), custom_call_target="tpu_custom_call" | custom-call | tf_op jit(solution)/shard_map/experts/pallas_call | solution.py:327
  98.1 4.5 %all-to-all-start.2 = ((bf16[128,48,128]{2,1,0:T(8,128)(2,1)}), bf16[128,48,128]{2,1,0:T(8,128)(2,1)S(1)}, u32[]{:S(2)}, u32[]{:S(2)}) async-start(bf16[128,48,128]{2,1,0:T(8,128)(2,1)} %experts.1), calls=%async_computation.2 | async-start | bytes 3145728 | tf_op jit(solution)/shard_map/all_to_all | solution.py:460
  102.9 1.2 copy-done.8
  104.1 1.2 copy-done.9
  105.4 0.7 shared.1.base
  106.1 21.6 %all-to-all-done.2 = bf16[128,48,128]{2,1,0:T(8,128)(2,1)S(1)} async-done(((bf16[128,48,128]{2,1,0:T(8,128)(2,1)}), bf16[128,48,128]{2,1,0:T(8,128)(2,1)S(1)}, u32[]{:S(2)}, u32[]{:S(2)}) %all-to-all-start.2) | async-done | bytes 1572896 | tf_op jit(solution)/shard_map/all_to_all | solution.py:460
  127.7 0.9 combine.1
  (55 shorter events, 3.5 us)
Async XLA Ops:
  0.6 9.7 %copy-start.6 = (s32[24]{0:T(128)S(1)}, s32[24]{0:T(128)}, u32[]{:S(2)}) copy-start(s32[24]{0:T(128)} %lengths.1) | copy-start | bytes 292
  0.6 9.7 %copy-start.12 = (bf16[2048]{0:T(1024)(128)(2,1)S(1)}, bf16[2048]{0:T(1024)(128)(2,1)}, u32[]{:S(2)}) copy-start(bf16[2048]{0:T(1024)(128)(2,1)} %param.30) | copy-start | bytes 12292
  0.7 10.3 %copy-start.14 = (bf16[256]{0:T(256)(128)(2,1)S(1)}, bf16[256]{0:T(256)(128)(2,1)}, u32[]{:S(2)}) copy-start(bf16[256]{0:T(256)(128)(2,1)} %param.32) | copy-start | bytes 1540
  0.7 10.9 %copy-start.15 = (bf16[256]{0:T(256)(128)(2,1)S(1)}, bf16[256]{0:T(256)(128)(2,1)}, u32[]{:S(2)}) copy-start(bf16[256]{0:T(256)(128)(2,1)} %param.36) | copy-start | bytes 1540
  0.7 11.6 %copy-start.5 = (bf16[24,2048]{1,0:T(8,128)(2,1)S(1)}, bf16[24,2048]{1,0:T(8,128)(2,1)}, u32[]{:S(2)}) copy-start(bf16[24,2048]{1,0:T(8,128)(2,1)} %tokens.3) | copy-start | bytes 294916
  2.7 26.0 %all-to-all-start = ((bf16[16,16,2048]{2,1,0:T(8,128)(2,1)}), bf16[16,16,2048]{2,1,0:T(8,128)(2,1)S(1)}, u32[]{:S(2)}, u32[]{:S(2)}) async-start(bf16[16,16,2048]{2,1,0:T(8,128)(2,1)} %broadcast_in_dim.18), calls=%async_computation | async-start | bytes 2097152 | tf_op jit(solution)/shard_map/all_to_all | solution.py:407
  12.3 25.6 %copy-start.10 = (s32[24,6]{0,1:T(8,128)S(1)}, s32[24,6]{0,1:T(8,128)}, u32[]{:S(2)}) copy-start(s32[24,6]{0,1:T(8,128)} %param.28) | copy-start | bytes 1732
  28.7 13.5 %collective-permute-start = (bf16[16,16,2048]{2,1,0:T(8,128)(2,1)S(1)}, bf16[16,16,2048]{2,1,0:T(8,128)(2,1)S(1)}, u32[]{:S(2)}, u32[]{:S(2)}) collective-permute-start(bf16[16,16,2048]{2,1,0:T(8,128)(2,1)S(1)} %all-to-all-done.mine), channel_id=1, source_target_pairs={{0,1},{1,0},{2,3},{3,2},{4,5},{5,4},{6,7},{7,6},{8,9},{9,8},{10,11... | collective-permute-start | bytes 3145736 | tf_op jit(solution)/shard_map/ppermute | solution.py:441
  29.7 4.6 %collective-permute-start.1 = (bf16[24,2048]{1,0:T(8,128)(2,1)S(1)}, bf16[24,2048]{1,0:T(8,128)(2,1)S(1)}, u32[]{:S(2)}, u32[]{:S(2)}) collective-permute-start(bf16[24,2048]{1,0:T(8,128)(2,1)S(1)} %get-tuple-element.13.v0), channel_id=1, source_target_pairs={{0,32},{32,0},{64,96},{96,64},{1,33},{33,1},{65,97},{97,65},{2,34}... | collective-permute-start | bytes 294920 | tf_op jit(solution)/shard_map/ppermute | solution.py:444
  34.4 15.5 %copy-start.13 = (bf16[2048]{0:T(1024)(128)(2,1)S(1)}, bf16[2048]{0:T(1024)(128)(2,1)}, u32[]{:S(2)}) copy-start(bf16[2048]{0:T(1024)(128)(2,1)} %param.41) | copy-start | bytes 12292
  34.4 7.8 %collective-permute-start.2 = (bf16[48,2048]{1,0:T(8,128)(2,1)S(1)}, bf16[48,2048]{1,0:T(8,128)(2,1)S(1)}, u32[]{:S(2)}, u32[]{:S(2)}) collective-permute-start(bf16[48,2048]{1,0:T(8,128)(2,1)S(1)} %pad_maximum_fusion), channel_id=1, source_target_pairs={{0,96},{96,0},{32,64},{64,32},{1,97},{97,1},{33,65},{65,33},{2,98}... | collective-permute-start | bytes 589832 | tf_op jit(solution)/shard_map/ppermute | solution.py:446
  42.2 1.0 copy-start.3
  43.2 1.2 copy-start.4
  44.4 46.9 %copy-start.1 = (bf16[1,2048,512]{2,1,0:T(8,128)(2,1)S(1)}, bf16[1,2048,512]{2,1,0:T(8,128)(2,1)}, u32[]{:S(2)}) copy-start(bf16[1,2048,512]{2,1,0:T(8,128)(2,1)} %up.2) | copy-start | bytes 6291460
  45.4 4.2 %collective-permute-start.3 = (bf16[48,512]{1,0:T(8,128)(2,1)S(1)}, bf16[48,512]{1,0:T(8,128)(2,1)S(1)}, u32[]{:S(2)}, u32[]{:S(2)}) collective-permute-start(bf16[48,512]{1,0:T(8,128)(2,1)S(1)} %slice.12), channel_id=1, source_target_pairs={{0,96},{96,0},{32,64},{64,32},{1,97},{97,1},{33,65},{65,33},{2,98}... | collective-permute-start | bytes 147464 | tf_op jit(solution)/shard_map/ppermute | solution.py:448
  49.6 3.0 %collective-permute-start.4 = (bf16[2,24,512]{2,1,0:T(8,128)(2,1)S(1)}, bf16[2,24,512]{2,1,0:T(8,128)(2,1)S(1)}, u32[]{:S(2)}, u32[]{:S(2)}) collective-permute-start(bf16[2,24,512]{2,1,0:T(8,128)(2,1)S(1)} %pad_maximum_fusion.1), channel_id=1, source_target_pairs={{0,32},{32,0},{64,96},{96,64},{1,33},{33,1},{65,97},{97,65},{2,34}... | collective-permute-start | bytes 147464 | tf_op jit(solution)/shard_map/ppermute | solution.py:449
  53.7 37.6 %copy-start = (bf16[1,2048,512]{2,1,0:T(8,128)(2,1)S(1)}, bf16[1,2048,512]{2,1,0:T(8,128)(2,1)}, u32[]{:S(2)}) copy-start(bf16[1,2048,512]{2,1,0:T(8,128)(2,1)} %gate.2) | copy-start | bytes 6291460
  91.3 1.6 %copy-start.2 = (bf16[1,512,2048]{2,1,0:T(8,128)(2,1)S(1)}, bf16[1,512,2048]{2,1,0:T(8,128)(2,1)}, u32[]{:S(2)}) copy-start(bf16[1,512,2048]{2,1,0:T(8,128)(2,1)} %down.2) | copy-start | bytes 6291460
  98.1 4.5 %copy-start.11 = (f32[24,6]{0,1:T(8,128)S(1)}, f32[24,6]{0,1:T(8,128)}, u32[]{:S(2)}) copy-start(f32[24,6]{0,1:T(8,128)} %param.29) | copy-start | bytes 1732
  98.1 4.8 %copy-start.7 = (bf16[2048,256]{1,0:T(8,128)(2,1)S(1)}, bf16[2048,256]{1,0:T(8,128)(2,1)}, u32[]{:S(2)}) copy-start(bf16[2048,256]{1,0:T(8,128)(2,1)} %gate.3) | copy-start | bytes 3145732
  98.1 29.5 %all-to-all-start.2 = ((bf16[128,48,128]{2,1,0:T(8,128)(2,1)}), bf16[128,48,128]{2,1,0:T(8,128)(2,1)S(1)}, u32[]{:S(2)}, u32[]{:S(2)}) async-start(bf16[128,48,128]{2,1,0:T(8,128)(2,1)} %experts.1), calls=%async_computation.2 | async-start | bytes 3145728 | tf_op jit(solution)/shard_map/all_to_all | solution.py:460
  102.9 1.2 copy-start.8
  104.1 1.2 copy-start.9
